TPU v7x, 32 devices: a whole 2x2x4 slice. The times are simulated.
32 devices in a mesh: gr: 2 (over x), sp: 8 (over z, y), tp: 2 (over core).
Axes of the slice: x: 2, y: 2, z: 4, core: 2. Of those that a mesh axis runs over, the one named last changes fastest.
Arguments:
- tokens: bfloat16 [2, 2, 6144, 2048], P('gr', 'tp', 'sp'), may hold values from -6 to 6
- key_weight: bfloat16 [2048, 2048], replicated, may hold values from -0.125 to 0.125
- value_weight: bfloat16 [2048, 2048], replicated, may hold values from -0.125 to 0.125
- cum_gate: float32 [2, 32, 2, 6144], P('gr', None, 'tp', 'sp'), may hold values from -12588 to 0, as said below
- query: bfloat16 [2, 32, 64], P('gr', 'sp'), may hold values from -12 to 12
Outputs:
- kv_cache: bfloat16 [2, 32, 12288, 128], P('gr', 'sp', 'tp')
- gate_cache: float32 [2, 32, 12288], P('gr', 'sp', 'tp')
- read: bfloat16 [2, 32, 64], P('gr', 'sp')
Inputs may be any that keep to these rules, and one draw needn't show every extreme that they name: `cum_gate`: each head's entries never rise along the positions.
All inputs are finite; a program needn't handle non-finite values.
Results may differ from a plain program's by a relative error of at most 0.012.
Values may be sent and summed in bfloat16 or wider, within the bound.
A program may use at most 128 MiB of HBM per device.

v0:
```python
import functools

import jax
import jax.numpy as jnp
from jax import lax
from jax.experimental import pallas as pl
from jax.experimental.pallas import tpu as pltpu
from jax.sharding import PartitionSpec as P

MESH = pl.DeviceIdType.MESH
LANES = 128


def partner(step, me, n):
    if n % 2:
        return lax.rem(me + 1 + step, n)
    turn, flip = step // 2, lax.rem(step, 2)
    flip = jnp.where(turn == n // 2 - 1, 1 - flip, flip)
    return lax.rem(me // 2 + 1 + turn, n // 2) * 2 + lax.rem(me + flip, 2)


def exchange_kernel(
    n, per_owner, tile, head,
    tokens, key_weight, value_weight, gates, query,
    kv, gate_in, result,
    rows, weights, outgoing, mine, theirs,
    row_sem, weight_sem, send_sem, recv_sem, gate_send, gate_recv, pair_sem,
):
    me = lax.axis_index("sp")
    core = lax.axis_index("tp")
    count = rows.shape[0]
    tiles = count // tile
    columns = weights.shape[3]
    group_heads = columns // head
    owners = group_heads // per_owner
    groups = n // owners

    def group_of(step):
        if owners == 1:
            return partner(step, me, n)
        return lax.rem(me // owners + 1 + step, groups)

    def load_rows(t):
        span = pl.ds(t * tile, tile)
        return pltpu.make_async_copy(tokens.at[span, :], rows.at[span, :], row_sem.at[t])

    def load_weight(step, which):
        at = pl.ds(pl.multiple_of(group_of(step) * columns, columns), columns)
        source = (key_weight, value_weight)[which]
        return pltpu.make_async_copy(
            source.at[:, at], weights.at[step, which], weight_sem.at[step, which]
        )

    load_rows(0).start()
    load_weight(0, 0).start()
    load_weight(0, 1).start()
    for t in range(1, tiles):
        load_rows(t).start()

    barrier = pltpu.get_barrier_semaphore()

    @pl.loop(1, n)
    def _(k):
        pl.semaphore_signal(
            barrier, inc=1, device_id={"sp": lax.rem(me + k, n)}, device_id_type=MESH
        )

    pl.semaphore_signal(barrier, inc=1, device_id={"tp": 1 - core}, device_id_type=MESH)
    pl.semaphore_wait(barrier, n)

    def gate_copy(owner):
        return pltpu.make_async_remote_copy(
            src_ref=gates.at[owner], dst_ref=gate_in.at[me],
            send_sem=gate_send.at[owner], recv_sem=gate_recv.at[me],
            device_id={"sp": owner}, device_id_type=MESH,
        )

    def gate_own():
        return pltpu.make_async_copy(gates.at[me], gate_in.at[me], gate_recv.at[me])

    @pl.loop(0, n - 1)
    def _(k):
        gate_copy(lax.rem(me + 1 + k, n)).start()

    gate_own().start()

    def block_copy(owner, t):
        return pltpu.make_async_remote_copy(
            src_ref=outgoing.at[owner, :, pl.ds(t * tile, tile), :],
            dst_ref=kv.at[:, pl.ds(pl.multiple_of(me * count + t * tile, tile), tile), :],
            send_sem=send_sem.at[owner, t], recv_sem=recv_sem.at[me, t],
            device_id={"sp": owner}, device_id_type=MESH,
        )

    def block_own(t):
        return pltpu.make_async_copy(
            outgoing.at[me, :, pl.ds(t * tile, tile), :],
            kv.at[:, pl.ds(pl.multiple_of(me * count + t * tile, tile), tile), :],
            recv_sem.at[me, t],
        )

    low = lax.broadcasted_iota(jnp.int32, (tile, LANES), 1) < head

    def project(step, first):
        group = group_of(step)

        if first:
            for ahead in range(1, min(3, groups)):
                load_weight(ahead, 0).start()
                load_weight(ahead, 1).start()
        else:
            @pl.when(step + 2 < groups)
            def _():
                load_weight(step + 2, 0).start()
                load_weight(step + 2, 1).start()

        load_weight(step, 0).wait()
        load_weight(step, 1).wait()
        for t in range(tiles):
            if first:
                load_rows(t).wait()
            left = rows[pl.ds(t * tile, tile), :]
            keys = jnp.dot(left, weights[step, 0], preferred_element_type=jnp.float32)
            values = jnp.dot(left, weights[step, 1], preferred_element_type=jnp.float32)
            for pair in range(columns // LANES):
                span = slice(pair * LANES, (pair + 1) * LANES)
                k, v = keys[:, span], values[:, span]
                joined = (
                    jnp.where(low, k, pltpu.roll(v, head, 1)),
                    jnp.where(low, pltpu.roll(k, head, 1), v),
                )
                for half in range(2):
                    local = pair * 2 + half
                    owner = group * owners + local // per_owner
                    outgoing[owner, local % per_owner, pl.ds(t * tile, tile), :] = joined[
                        half
                    ].astype(jnp.bfloat16)
            for j in range(owners):
                owner = group * owners + j

                @pl.when(owner != me)
                def _():
                    block_copy(owner, t).start()

                @pl.when(owner == me)
                def _():
                    block_own(t).start()

    project(0, True)

    def later(step, carry):
        project(step, False)
        return carry

    lax.fori_loop(1, groups, later, 0)

    wide = jnp.concatenate(
        [query[...].astype(jnp.float32), jnp.zeros((per_owner, LANES - head), jnp.float32)], axis=1
    ) * (head ** -0.5)
    head_row = lax.broadcasted_iota(jnp.int32, (per_owner, LANES), 0)
    tile_row = lax.broadcasted_iota(jnp.int32, (per_owner, tile), 0)
    queries = [jnp.where(head_row == h, wide, 0.0).astype(jnp.bfloat16) for h in range(per_owner)]

    @pl.loop(0, n - 1)
    def _(k):
        source = lax.rem(me + 1 + k, n)
        gate_copy(source).wait_send()
        pltpu.make_async_copy(gates.at[source], gate_in.at[source], gate_recv.at[source]).wait()

    gate_own().wait()

    def read_block(source, t, carry):
        top, total, weighted = carry
        span = pl.ds(pl.multiple_of(source * count + t * tile, tile), tile)
        pltpu.make_async_copy(
            outgoing.at[me, :, pl.ds(t * tile, tile), :], kv.at[:, span, :], recv_sem.at[source, t]
        ).wait()
        scores = None
        blocks = [kv[h, span, :] for h in range(per_owner)]
        for h in range(per_owner):
            term = lax.dot_general(
                queries[h], blocks[h], (((1,), (1,)), ((), ())), preferred_element_type=jnp.float32
            )
            scores = term if scores is None else scores + term
        gate = jnp.concatenate(
            [gate_in[source, h, :, pl.ds(t * tile, tile)] for h in range(per_owner)], axis=0
        )
        scores = scores - gate
        new_top = jnp.maximum(top, jnp.max(scores, axis=1, keepdims=True))
        scale = jnp.exp(top - new_top)
        probs = jnp.exp(scores - new_top)
        total = total * scale + jnp.sum(probs, axis=1, keepdims=True)
        weighted = weighted * scale
        for h in range(per_owner):
            picked = jnp.where(tile_row == h, probs, 0.0).astype(jnp.bfloat16)
            weighted = weighted + jnp.dot(picked, blocks[h], preferred_element_type=jnp.float32)
        return new_top, total, weighted

    carry = (
        jnp.full((per_owner, 1), -1e30, jnp.float32),
        jnp.zeros((per_owner, 1), jnp.float32),
        jnp.zeros((per_owner, LANES), jnp.float32),
    )

    for t in range(tiles):
        def from_source(k, carry, t=t):
            return read_block(partner(n - 1 - k, me, n), t, carry)

        carry = lax.fori_loop(0, n, from_source, carry)

    top, total, weighted = carry
    lane = lax.broadcasted_iota(jnp.int32, (per_owner, LANES), 1)
    packed = jnp.where(lane < head // 2, top, jnp.where(lane < head, total, weighted))
    mine[...] = packed
    swap = pltpu.make_async_remote_copy(
        src_ref=mine, dst_ref=theirs, send_sem=pair_sem.at[0], recv_sem=pair_sem.at[1],
        device_id={"tp": 1 - core}, device_id_type=MESH,
    )
    swap.start()

    @pl.loop(0, n - 1)
    def _(k):
        for t in range(tiles):
            block_copy(lax.rem(me + 1 + k, n), t).wait_send()

    swap.wait()
    other = theirs[...]
    one = jnp.where(core == 0, packed, other)
    two = jnp.where(core == 0, other, packed)
    top_one, top_two = one[:, :1], two[:, :1]
    joint = jnp.maximum(top_one, top_two)
    scale_one, scale_two = jnp.exp(top_one - joint), jnp.exp(top_two - joint)
    at = head // 2
    bottom = one[:, at:at + 1] * scale_one + two[:, at:at + 1] * scale_two
    result[...] = (one * scale_one + two * scale_two) / bottom


def finish_kernel(head, kv, gate_in, result, kv_out, gate_out, read, sem):
    heads, length = kv.shape[0], kv.shape[1]
    copies = [
        pltpu.make_async_copy(kv.at[h], kv_out.at[h], sem.at[h]) for h in range(heads)
    ]
    for copy in copies:
        copy.start()
    n, count = gate_in.shape[0], gate_in.shape[3]
    for source in range(n):
        gate_out[:, source * count:(source + 1) * count] = jnp.concatenate(
            [gate_in[source, h] for h in range(heads)], axis=0
        )
    read[...] = pltpu.roll(result[...], head, 1)[:, :head].astype(jnp.bfloat16)
    for copy in copies:
        copy.wait()


def on_device(n, tokens, key_weight, value_weight, cum_gate, query):
    _, _, count, width = tokens.shape
    heads = cum_gate.shape[1]
    per_owner, head = query.shape[1], query.shape[2]
    tile = 256 if count % 256 == 0 else count
    columns = max(per_owner * head, LANES)
    groups = heads * head // columns
    tiles = count // tile
    any_space = pl.BlockSpec(memory_space=pl.ANY)
    vmem = pl.BlockSpec(memory_space=pltpu.VMEM)
    kv, gate_in, result = pl.pallas_call(
        functools.partial(exchange_kernel, n, per_owner, tile, head),
        name="exchange",
        out_shape=(
            pltpu.VMEM((per_owner, n * count, 2 * head), jnp.bfloat16),
            pltpu.VMEM((n, per_owner, 1, count), jnp.float32),
            pltpu.VMEM((per_owner, 2 * head), jnp.float32),
        ),
        in_specs=[any_space] * 4 + [vmem],
        out_specs=(vmem, vmem, vmem),
        scratch_shapes=[
            pltpu.VMEM((count, width), jnp.bfloat16),
            pltpu.VMEM((groups, 2, width, columns), jnp.bfloat16),
            pltpu.VMEM((n, per_owner, count, 2 * head), jnp.bfloat16),
            pltpu.VMEM((per_owner, 2 * head), jnp.float32),
            pltpu.VMEM((per_owner, 2 * head), jnp.float32),
            pltpu.SemaphoreType.DMA((tiles,)),
            pltpu.SemaphoreType.DMA((groups, 2)),
            pltpu.SemaphoreType.DMA((n, tiles)),
            pltpu.SemaphoreType.DMA((n, tiles)),
            pltpu.SemaphoreType.DMA((n,)),
            pltpu.SemaphoreType.DMA((n,)),
            pltpu.SemaphoreType.DMA((2,)),
        ],
        compiler_params=pltpu.CompilerParams(
            collective_id=0, has_side_effects=True, vmem_limit_bytes=56 * 1024 * 1024
        ),
    )(
        tokens.reshape(count, width),
        key_weight,
        value_weight,
        cum_gate.reshape(n, per_owner, 1, count),
        query.reshape(per_owner, head),
    )
    kv_out, gate_out, read = pl.pallas_call(
        functools.partial(finish_kernel, head),
        name="finish",
        out_shape=(
            jax.ShapeDtypeStruct((per_owner, n * count, 2 * head), jnp.bfloat16),
            jax.ShapeDtypeStruct((per_owner, n * count), jnp.float32),
            jax.ShapeDtypeStruct((per_owner, head), jnp.bfloat16),
        ),
        in_specs=[vmem, vmem, vmem],
        out_specs=(any_space, vmem, vmem),
        scratch_shapes=[pltpu.SemaphoreType.DMA((per_owner,))],
        compiler_params=pltpu.CompilerParams(vmem_limit_bytes=16 * 1024 * 1024),
    )(kv, gate_in, result)
    return kv_out[None], gate_out[None], read[None]


def solution(mesh):
    placed = (P("gr", "tp", "sp", None), P(), P(), P("gr", None, "tp", "sp"), P("gr", "sp", None))
    return jax.shard_map(
        functools.partial(on_device, mesh.shape["sp"]),
        mesh=mesh,
        in_specs=placed,
        out_specs=(P("gr", "sp", "tp", None), P("gr", "sp", "tp"), P("gr", "sp", None)),
        check_vma=False,
    )
```

profile of v0, /device:TPU:11, one launch (start us, length us, event | category | flops | bytes accessed | tf_op | source)
XLA Modules:
  0.0 150.4 jit_solution(14540696441196388960)
XLA Ops:
  0.6 146.3 %exchange.1 = (bf16[4,6144,128]{2,1,0:T(8,128)(2,1)S(1)}, f32[8,4,1,768]{3,2,1,0:T(1,128)S(1)}, f32[4,128]{1,0:T(4,128)S(1)}) custom-call(bf16[768,2048]{1,0:T(8,128)(2,1)} %bitcast.6, bf16[2048,2048]{1,0:T(8,128)(2,1)} %key_weight.1, bf16[2048,2048]{1,0:T(8,128)(2,1)} %value_weight.1, f32[8,4,1,768]{3,2,1,0:T(1,128)} %bitcast.7, bf16[4,64]{1,0:T(4,128)(2,1)} %bitcast.8), custom_call_target="tpu_custom_call" | custom-call | tf_op jit(solution)/shard_map/exchange/pallas_call | solution.py:265
  147.0 3.4 %finish.1 = (bf16[4,6144,128]{2,1,0:T(8,128)(2,1)}, f32[4,6144]{1,0:T(4,128)}, bf16[4,64]{1,0:T(4,128)(2,1)}) custom-call(bf16[4,6144,128]{2,1,0:T(8,128)(2,1)S(1)} %get-tuple-element.9.kv, f32[8,4,1,768]{3,2,1,0:T(1,128)S(1)} %get-tuple-element.10.gate_in, f32[4,128]{1,0:T(4,128)S(1)} %get-tuple-element.11.result), custom_call_target="tpu_custom_call" | custom-call | tf_op jit(solution)/shard_map/finish/pallas_call | solution.py:299
where the time goes:
time: 151 us; the launch traced here: 150 us
  Pallas kernels  150 us (99%)
    pallas_call x1, Pallas kernels, on_device(): pl.pallas_call(functools.partial(exchange_kernel, n, per_owner, tile, hea...  146 us
    pallas_call x1, Pallas kernels, on_device(): pl.pallas_call(functools.partial(finish_kernel, head), name='finish', out...  3.41 us

commit v1 on v0

v1 whole, which is shorter than its diff:
```python
import functools

import jax
import jax.numpy as jnp
from jax import lax
from jax.experimental import pallas as pl
from jax.experimental.pallas import tpu as pltpu
from jax.sharding import PartitionSpec as P

MESH = pl.DeviceIdType.MESH
LANES = 128


def partner(step, me, n):
    if n % 2:
        return lax.rem(me + 1 + step, n)
    turn, flip = step // 2, lax.rem(step, 2)
    flip = jnp.where(turn == n // 2 - 1, 1 - flip, flip)
    return lax.rem(me // 2 + 1 + turn, n // 2) * 2 + lax.rem(me + flip, 2)


def exchange_kernel(
    n, per_owner, tile, head,
    tokens, key_weight, value_weight, gates, query,
    kv, gate_out, read,
    rows, weights, outgoing, gate_own, gate_send, gate_in, query_own, query_in, part_send, part_in, mine, theirs,
    row_sem, weight_sem, small_sem, send_sem, recv_sem,
    gate_sent, gate_recv, query_sent, query_recv, part_sent, part_recv, pair_sem,
):
    me = lax.axis_index("sp")
    core = lax.axis_index("tp")
    count = rows.shape[0]
    tiles = count // tile
    early = max(tiles - 1, 1)
    columns = weights.shape[3]
    group_heads = columns // head
    owners = group_heads // per_owner
    groups = n // owners

    def group_of(step):
        if owners == 1:
            return partner(step, me, n)
        return lax.rem(me // owners + 1 + step, groups)

    def load_rows(t):
        span = pl.ds(t * tile, tile)
        return pltpu.make_async_copy(tokens.at[span, :], rows.at[span, :], row_sem.at[t])

    def load_weight(step, which):
        at = pl.ds(pl.multiple_of(group_of(step) * columns, columns), columns)
        source = (key_weight, value_weight)[which]
        return pltpu.make_async_copy(
            source.at[:, at], weights.at[step, which], weight_sem.at[step, which]
        )

    load_query = pltpu.make_async_copy(query, query_own, small_sem.at[0])
    load_gates = pltpu.make_async_copy(gates, gate_own, small_sem.at[1])
    load_query.start()
    load_rows(0).start()
    load_weight(0, 0).start()
    load_weight(0, 1).start()
    load_gates.start()
    for t in range(1, tiles):
        load_rows(t).start()

    barrier = pltpu.get_barrier_semaphore()

    @pl.loop(1, n)
    def _(k):
        pl.semaphore_signal(
            barrier, inc=1, device_id={"sp": lax.rem(me + k, n)}, device_id_type=MESH
        )

    pl.semaphore_signal(barrier, inc=1, device_id={"tp": 1 - core}, device_id_type=MESH)

    load_query.wait()
    wide = jnp.concatenate(
        [query_own[...].astype(jnp.float32), jnp.zeros((per_owner, LANES - head), jnp.float32)], axis=1
    ) * (head ** -0.5)
    query_in[me] = wide

    def query_copy(owner):
        return pltpu.make_async_remote_copy(
            src_ref=query_in.at[me], dst_ref=query_in.at[me],
            send_sem=query_sent.at[owner], recv_sem=query_recv.at[me],
            device_id={"sp": owner}, device_id_type=MESH,
        )

    def gate_copy(owner):
        return pltpu.make_async_remote_copy(
            src_ref=gate_send.at[owner], dst_ref=gate_in.at[me],
            send_sem=gate_sent.at[owner], recv_sem=gate_recv.at[me],
            device_id={"sp": owner}, device_id_type=MESH,
        )

    def part_copy(owner):
        return pltpu.make_async_remote_copy(
            src_ref=part_send.at[owner], dst_ref=part_in.at[me],
            send_sem=part_sent.at[owner], recv_sem=part_recv.at[me],
            device_id={"sp": owner}, device_id_type=MESH,
        )

    def block_copy(owner, t):
        return pltpu.make_async_remote_copy(
            src_ref=outgoing.at[owner, :, pl.ds(t * tile, tile), :],
            dst_ref=kv.at[:, pl.ds(pl.multiple_of(me * count + t * tile, tile), tile), :],
            send_sem=send_sem.at[owner, t], recv_sem=recv_sem.at[me, t],
            device_id={"sp": owner}, device_id_type=MESH,
        )

    def block_own(t):
        return pltpu.make_async_copy(
            outgoing.at[me, :, pl.ds(t * tile, tile), :],
            kv.at[:, pl.ds(pl.multiple_of(me * count + t * tile, tile), tile), :],
            recv_sem.at[me, t],
        )

    def send_block(owner, t):
        @pl.when(owner != me)
        def _():
            block_copy(owner, t).start()

        @pl.when(owner == me)
        def _():
            block_own(t).start()

    def own_gates(owner, span):
        return jnp.concatenate([gate_own[owner, h, :, span] for h in range(per_owner)], axis=0)

    low = lax.broadcasted_iota(jnp.int32, (tile, LANES), 1) < head

    def open_links():
        load_gates.wait()

        @pl.loop(0, n)
        def _(k):
            gate_send[k] = own_gates(k, slice(None)).astype(jnp.bfloat16)

        gate_in[me] = own_gates(me, slice(None)).astype(jnp.bfloat16)
        pl.semaphore_wait(barrier, n)

        @pl.loop(0, n - 1)
        def _(k):
            owner = partner(k, me, n)
            gate_copy(owner).start()
            query_copy(owner).start()

    def project(step, first):
        group = group_of(step)

        if first:
            for ahead in range(1, min(3, groups)):
                load_weight(ahead, 0).start()
                load_weight(ahead, 1).start()
        else:
            @pl.when(step + 2 < groups)
            def _():
                load_weight(step + 2, 0).start()
                load_weight(step + 2, 1).start()

        load_weight(step, 0).wait()
        load_weight(step, 1).wait()
        for t in range(tiles):
            if first:
                load_rows(t).wait()
            left = rows[pl.ds(t * tile, tile), :]
            keys = jnp.dot(left, weights[step, 0], preferred_element_type=jnp.float32)
            values = jnp.dot(left, weights[step, 1], preferred_element_type=jnp.float32)
            for pair in range(columns // LANES):
                span = slice(pair * LANES, (pair + 1) * LANES)
                k, v = keys[:, span], values[:, span]
                joined = (
                    jnp.where(low, k, pltpu.roll(v, head, 1)),
                    jnp.where(low, pltpu.roll(k, head, 1), v),
                )
                for half in range(2):
                    local = pair * 2 + half
                    owner = group * owners + local // per_owner
                    outgoing[owner, local % per_owner, pl.ds(t * tile, tile), :] = joined[
                        half
                    ].astype(jnp.bfloat16)
            if first and t == 0:
                open_links()
            if t < early:
                for j in range(owners):
                    send_block(group * owners + j, t)

    project(0, True)

    def later(step, carry):
        project(step, False)
        return carry

    lax.fori_loop(1, groups, later, 0)

    @pl.loop(0, n - 1)
    def _(k):
        source = partner(k, me, n)
        query_copy(source).wait_send()
        pltpu.make_async_copy(query_in.at[source], query_in.at[source], query_recv.at[source]).wait()

    head_row = lax.broadcasted_iota(jnp.int32, (per_owner, LANES), 0)
    tile_row = lax.broadcasted_iota(jnp.int32, (per_owner, tile), 0)
    lane = lax.broadcasted_iota(jnp.int32, (per_owner, LANES), 1)

    def read_own(k, carry):
        owner = partner(k, me, n)
        asked = query_in[owner]
        queries = [
            jnp.where(head_row == h, asked, 0.0).astype(jnp.bfloat16) for h in range(per_owner)
        ]
        top = jnp.full((per_owner, 1), -1e30, jnp.float32)
        total = jnp.zeros((per_owner, 1), jnp.float32)
        weighted = jnp.zeros((per_owner, LANES), jnp.float32)
        for t in range(tiles):
            span = pl.ds(t * tile, tile)
            blocks = [outgoing[owner, h, span, :] for h in range(per_owner)]
            scores = None
            for h in range(per_owner):
                term = lax.dot_general(
                    queries[h], blocks[h], (((1,), (1,)), ((), ())), preferred_element_type=jnp.float32
                )
                scores = term if scores is None else scores + term
            scores = scores - own_gates(owner, span)
            new_top = jnp.maximum(top, jnp.max(scores, axis=1, keepdims=True))
            scale = jnp.exp(top - new_top)
            probs = jnp.exp(scores - new_top)
            total = total * scale + jnp.sum(probs, axis=1, keepdims=True)
            weighted = weighted * scale
            for h in range(per_owner):
                picked = jnp.where(tile_row == h, probs, 0.0).astype(jnp.bfloat16)
                weighted = weighted + jnp.dot(picked, blocks[h], preferred_element_type=jnp.float32)
            top = new_top
        packed = jnp.where(lane < head // 2, top, jnp.where(lane < head, total, weighted))
        part_send[owner] = packed

        @pl.when(owner != me)
        def _():
            part_copy(owner).start()

        return carry

    lax.fori_loop(0, n, read_own, 0)

    if early < tiles:
        @pl.loop(0, n)
        def _(k):
            owner = partner(k, me, n)
            for t in range(early, tiles):
                send_block(owner, t)

    @pl.loop(0, n - 1)
    def _(k):
        source = partner(k, me, n)
        gate_copy(source).wait_send()
        pltpu.make_async_copy(gate_in.at[source], gate_in.at[source], gate_recv.at[source]).wait()

    for source in range(n):
        gate_out[:, source * count:(source + 1) * count] = gate_in[source].astype(jnp.float32)

    def merge(one, two):
        top_one, top_two = one[:, :1], two[:, :1]
        joint = jnp.maximum(top_one, top_two)
        both = one * jnp.exp(top_one - joint) + two * jnp.exp(top_two - joint)
        return jnp.where(lane < head // 2, joint, both)

    def gather(k, carry):
        source = partner(k, me, n)
        part_copy(source).wait_send()
        pltpu.make_async_copy(part_in.at[source], part_in.at[source], part_recv.at[source]).wait()
        return merge(carry, part_in[source])

    packed = lax.fori_loop(0, n - 1, gather, part_send[me])
    mine[...] = packed
    swap = pltpu.make_async_remote_copy(
        src_ref=mine, dst_ref=theirs, send_sem=pair_sem.at[0], recv_sem=pair_sem.at[1],
        device_id={"tp": 1 - core}, device_id_type=MESH,
    )
    swap.start()
    swap.wait()
    other = theirs[...]
    joint = merge(jnp.where(core == 0, packed, other), jnp.where(core == 0, other, packed))
    at = head // 2
    answer = joint / joint[:, at:at + 1]
    read[...] = pltpu.roll(answer, head, 1)[:, :head].astype(jnp.bfloat16)

    for t in range(tiles):
        block_own(t).wait()

        @pl.loop(0, n - 1)
        def _(k, t=t):
            source = partner(n - 2 - k, me, n)
            block_copy(source, t).wait_send()
            pltpu.make_async_copy(
                kv.at[:, pl.ds(t * tile, tile), :], kv.at[:, pl.ds(t * tile, tile), :], recv_sem.at[source, t]
            ).wait()


def finish_kernel(pieces, kv, gates, answer, kv_out, gate_out, read, sem):
    heads, length = kv.shape[0], kv.shape[1]
    part = length // pieces
    copies = [
        pltpu.make_async_copy(
            kv.at[h, pl.ds(p * part, part), :], kv_out.at[h, pl.ds(p * part, part), :], sem.at[h * pieces + p]
        )
        for p in range(pieces)
        for h in range(heads)
    ]
    copies.append(pltpu.make_async_copy(gates, gate_out, sem.at[heads * pieces]))
    copies.append(pltpu.make_async_copy(answer, read, sem.at[heads * pieces + 1]))
    for copy in copies:
        copy.start()
    for copy in copies:
        copy.wait()


def on_device(n, tokens, key_weight, value_weight, cum_gate, query):
    _, _, count, width = tokens.shape
    heads = cum_gate.shape[1]
    per_owner, head = query.shape[1], query.shape[2]
    tile = 256 if count % 256 == 0 else count
    columns = max(per_owner * head, LANES)
    groups = heads * head // columns
    tiles = count // tile
    any_space = pl.BlockSpec(memory_space=pl.ANY)
    vmem = pl.BlockSpec(memory_space=pltpu.VMEM)
    kv, gates, answer = pl.pallas_call(
        functools.partial(exchange_kernel, n, per_owner, tile, head),
        name="exchange",
        out_shape=(
            pltpu.VMEM((per_owner, n * count, 2 * head), jnp.bfloat16),
            pltpu.VMEM((per_owner, n * count), jnp.float32),
            pltpu.VMEM((per_owner, head), jnp.bfloat16),
        ),
        in_specs=[any_space] * 5,
        out_specs=(vmem, vmem, vmem),
        scratch_shapes=[
            pltpu.VMEM((count, width), jnp.bfloat16),
            pltpu.VMEM((groups, 2, width, columns), jnp.bfloat16),
            pltpu.VMEM((n, per_owner, count, 2 * head), jnp.bfloat16),
            pltpu.VMEM((n, per_owner, 1, count), jnp.float32),
            pltpu.VMEM((n, per_owner, count), jnp.bfloat16),
            pltpu.VMEM((n, per_owner, count), jnp.bfloat16),
            pltpu.VMEM((per_owner, head), jnp.bfloat16),
            pltpu.VMEM((n, per_owner, LANES), jnp.float32),
            pltpu.VMEM((n, per_owner, LANES), jnp.float32),
            pltpu.VMEM((n, per_owner, LANES), jnp.float32),
            pltpu.VMEM((per_owner, LANES), jnp.float32),
            pltpu.VMEM((per_owner, LANES), jnp.float32),
            pltpu.SemaphoreType.DMA((tiles,)),
            pltpu.SemaphoreType.DMA((groups, 2)),
            pltpu.SemaphoreType.DMA((2,)),
            pltpu.SemaphoreType.DMA((n, tiles)),
            pltpu.SemaphoreType.DMA((n, tiles)),
            pltpu.SemaphoreType.DMA((n,)),
            pltpu.SemaphoreType.DMA((n,)),
            pltpu.SemaphoreType.DMA((n,)),
            pltpu.SemaphoreType.DMA((n,)),
            pltpu.SemaphoreType.DMA((n,)),
            pltpu.SemaphoreType.DMA((n,)),
            pltpu.SemaphoreType.DMA((2,)),
        ],
        compiler_params=pltpu.CompilerParams(
            collective_id=0, has_side_effects=True, vmem_limit_bytes=56 * 1024 * 1024
        ),
    )(
        tokens.reshape(count, width),
        key_weight,
        value_weight,
        cum_gate.reshape(n, per_owner, 1, count),
        query.reshape(per_owner, head),
    )
    pieces = 4 if n % 4 == 0 else 1
    kv_out, gate_out, read = pl.pallas_call(
        functools.partial(finish_kernel, pieces),
        name="finish",
        out_shape=(
            jax.ShapeDtypeStruct((per_owner, n * count, 2 * head), jnp.bfloat16),
            jax.ShapeDtypeStruct((per_owner, n * count), jnp.float32),
            jax.ShapeDtypeStruct((per_owner, head), jnp.bfloat16),
        ),
        in_specs=[vmem, vmem, vmem],
        out_specs=(any_space, any_space, any_space),
        scratch_shapes=[pltpu.SemaphoreType.DMA((per_owner * pieces + 2,))],
        compiler_params=pltpu.CompilerParams(vmem_limit_bytes=16 * 1024 * 1024),
    )(kv, gates, answer)
    return kv_out[None], gate_out[None], read[None]


def solution(mesh):
    placed = (P("gr", "tp", "sp", None), P(), P(), P("gr", None, "tp", "sp"), P("gr", "sp", None))
    return jax.shard_map(
        functools.partial(on_device, mesh.shape["sp"]),
        mesh=mesh,
        in_specs=placed,
        out_specs=(P("gr", "sp", "tp", None), P("gr", "sp", "tp"), P("gr", "sp", None)),
        check_vma=False,
    )
```

time: 151 us -> 149 us (0.987)
  Pallas kernels: 150 us -> 148 us
where the time goes in v1:
time: 149 us
  Pallas kernels  148 us (99%)
    pallas_call x1, Pallas kernels, on_device(): pl.pallas_call(functools.partial(exchange_kernel, n, per_owner, tile, hea...  145 us

profile of v1, /device:TPU:11, one launch (start us, length us, event | category | flops | bytes accessed | tf_op | source)
XLA Modules:
  0.0 148.8 jit_solution(4020857407842320994)
XLA Ops:
  0.6 145.4 %exchange.1 = (bf16[4,6144,128]{2,1,0:T(8,128)(2,1)S(1)}, f32[4,6144]{1,0:T(4,128)S(1)}, bf16[4,64]{1,0:T(4,128)(2,1)S(1)}) custom-call(bf16[768,2048]{1,0:T(8,128)(2,1)} %bitcast.6, bf16[2048,2048]{1,0:T(8,128)(2,1)} %key_weight.1, bf16[2048,2048]{1,0:T(8,128)(2,1)} %value_weight.1, f32[8,4,1,768]{3,2,1,0:T(1,128)} %bitcast.7, bf16[4,64]{1,0:T(4,128)(2,1)} %bitcast.8), custom_call_target="tpu_custom_call" | custom-call | tf_op jit(solution)/shard_map/exchange/pallas_call | solution.py:327
  146.0 2.8 %finish.1 = (bf16[4,6144,128]{2,1,0:T(8,128)(2,1)}, f32[4,6144]{1,0:T(4,128)}, bf16[4,64]{1,0:T(4,128)(2,1)}) custom-call(bf16[4,6144,128]{2,1,0:T(8,128)(2,1)S(1)} %get-tuple-element.9.kv, f32[4,6144]{1,0:T(4,128)S(1)} %get-tuple-element.10.gates, bf16[4,64]{1,0:T(4,128)(2,1)S(1)} %get-tuple-element.11.answer), custom_call_target="tpu_custom_call" | custom-call | tf_op jit(solution)/shard_map/finish/pallas_call | solution.py:374

commit v2 on v1

--- a/solution.py
+++ b/solution.py
@@ -11,19 +11,23 @@
 LANES = 128
 
 
-def partner(step, me, n):
-    if n % 2:
-        return lax.rem(me + 1 + step, n)
-    turn, flip = step // 2, lax.rem(step, 2)
-    flip = jnp.where(turn == n // 2 - 1, 1 - flip, flip)
-    return lax.rem(me // 2 + 1 + turn, n // 2) * 2 + lax.rem(me + flip, 2)
+def partner(step, me, n, turned=0):
+    turn, flip = step // 2, lax.rem(step + turned, 2)
+    flip = jnp.where(turn == n // 2 - 1, 1 - lax.rem(step, 2), flip)
+    half = n // 4
+    at = me // 2
+    far = at >= half
+    w = jnp.where(far, 2 * half - 1 - at, at)
+    goal = jnp.where(turn < half, 2 * half - 1 - turn, lax.rem(w + 1 + turn, half))
+    goal = jnp.where(far, 2 * half - 1 - goal, goal)
+    return goal * 2 + lax.rem(me + flip, 2)
 
 
 def exchange_kernel(
     n, per_owner, tile, head,
     tokens, key_weight, value_weight, gates, query,
-    kv, gate_out, read,
-    rows, weights, outgoing, gate_own, gate_send, gate_in, query_own, query_in, part_send, part_in, mine, theirs,
+    kv, outgoing, gate_out, read,
+    rows, weights, gate_own, gate_send, gate_in, query_own, query_in, part_send, part_in, mine, theirs,
     row_sem, weight_sem, small_sem, send_sem, recv_sem,
     gate_sent, gate_recv, query_sent, query_recv, part_sent, part_recv, pair_sem,
 ):
@@ -39,7 +43,7 @@
 
     def group_of(step):
         if owners == 1:
-            return partner(step, me, n)
+            return partner(step, me, n, core)
         return lax.rem(me // owners + 1 + step, groups)
 
     def load_rows(t):
@@ -73,12 +77,6 @@
 
     pl.semaphore_signal(barrier, inc=1, device_id={"tp": 1 - core}, device_id_type=MESH)
 
-    load_query.wait()
-    wide = jnp.concatenate(
-        [query_own[...].astype(jnp.float32), jnp.zeros((per_owner, LANES - head), jnp.float32)], axis=1
-    ) * (head ** -0.5)
-    query_in[me] = wide
-
     def query_copy(owner):
         return pltpu.make_async_remote_copy(
             src_ref=query_in.at[me], dst_ref=query_in.at[me],
@@ -130,81 +128,37 @@
     low = lax.broadcasted_iota(jnp.int32, (tile, LANES), 1) < head
 
     def open_links():
+        pl.semaphore_wait(barrier, n)
+
+    def send_queries():
         load_gates.wait()
-
-        @pl.loop(0, n)
+        load_query.wait()
+        query_in[me] = jnp.concatenate(
+            [query_own[...].astype(jnp.float32), jnp.zeros((per_owner, LANES - head), jnp.float32)], axis=1
+        ) * (head ** -0.5)
+
+        @pl.loop(0, n - 1)
         def _(k):
-            gate_send[k] = own_gates(k, slice(None)).astype(jnp.bfloat16)
-
-        gate_in[me] = own_gates(me, slice(None)).astype(jnp.bfloat16)
-        pl.semaphore_wait(barrier, n)
-
+            query_copy(partner(k, me, n)).start()
+
+    def send_gates():
         @pl.loop(0, n - 1)
         def _(k):
             owner = partner(k, me, n)
+            gate_send[owner] = own_gates(owner, slice(None)).astype(jnp.bfloat16)
             gate_copy(owner).start()
-            query_copy(owner).start()
-
-    def project(step, first):
-        group = group_of(step)
-
-        if first:
-            for ahead in range(1, min(3, groups)):
-                load_weight(ahead, 0).start()
-                load_weight(ahead, 1).start()
-        else:
-            @pl.when(step + 2 < groups)
-            def _():
-                load_weight(step + 2, 0).start()
-                load_weight(step + 2, 1).start()
-
-        load_weight(step, 0).wait()
-        load_weight(step, 1).wait()
-        for t in range(tiles):
-            if first:
-                load_rows(t).wait()
-            left = rows[pl.ds(t * tile, tile), :]
-            keys = jnp.dot(left, weights[step, 0], preferred_element_type=jnp.float32)
-            values = jnp.dot(left, weights[step, 1], preferred_element_type=jnp.float32)
-            for pair in range(columns // LANES):
-                span = slice(pair * LANES, (pair + 1) * LANES)
-                k, v = keys[:, span], values[:, span]
-                joined = (
-                    jnp.where(low, k, pltpu.roll(v, head, 1)),
-                    jnp.where(low, pltpu.roll(k, head, 1), v),
-                )
-                for half in range(2):
-                    local = pair * 2 + half
-                    owner = group * owners + local // per_owner
-                    outgoing[owner, local % per_owner, pl.ds(t * tile, tile), :] = joined[
-                        half
-                    ].astype(jnp.bfloat16)
-            if first and t == 0:
-                open_links()
-            if t < early:
-                for j in range(owners):
-                    send_block(group * owners + j, t)
-
-    project(0, True)
-
-    def later(step, carry):
-        project(step, False)
-        return carry
-
-    lax.fori_loop(1, groups, later, 0)
-
-    @pl.loop(0, n - 1)
-    def _(k):
-        source = partner(k, me, n)
-        query_copy(source).wait_send()
-        pltpu.make_async_copy(query_in.at[source], query_in.at[source], query_recv.at[source]).wait()
+
+        gate_in[me] = own_gates(me, slice(None)).astype(jnp.bfloat16)
 
     head_row = lax.broadcasted_iota(jnp.int32, (per_owner, LANES), 0)
     tile_row = lax.broadcasted_iota(jnp.int32, (per_owner, tile), 0)
     lane = lax.broadcasted_iota(jnp.int32, (per_owner, LANES), 1)
 
-    def read_own(k, carry):
-        owner = partner(k, me, n)
+    def read_own(owner):
+        @pl.when(owner != me)
+        def _():
+            pltpu.make_async_copy(query_in.at[owner], query_in.at[owner], query_recv.at[owner]).wait()
+
         asked = query_in[owner]
         queries = [
             jnp.where(head_row == h, asked, 0.0).astype(jnp.bfloat16) for h in range(per_owner)
@@ -238,21 +192,72 @@
         def _():
             part_copy(owner).start()
 
+    def project(step, first):
+        group = group_of(step)
+
+        if first:
+            for ahead in range(1, min(3, groups)):
+                load_weight(ahead, 0).start()
+                load_weight(ahead, 1).start()
+        else:
+            @pl.when(step + 2 < groups)
+            def _():
+                load_weight(step + 2, 0).start()
+                load_weight(step + 2, 1).start()
+
+        load_weight(step, 0).wait()
+        load_weight(step, 1).wait()
+        for t in range(tiles):
+            if first:
+                load_rows(t).wait()
+            left = rows[pl.ds(t * tile, tile), :]
+            keys = jnp.dot(left, weights[step, 0], preferred_element_type=jnp.float32)
+            values = jnp.dot(left, weights[step, 1], preferred_element_type=jnp.float32)
+            for pair in range(columns // LANES):
+                span = slice(pair * LANES, (pair + 1) * LANES)
+                k, v = keys[:, span], values[:, span]
+                joined = (
+                    jnp.where(low, k, pltpu.roll(v, head, 1)),
+                    jnp.where(low, pltpu.roll(k, head, 1), v),
+                )
+                for half in range(2):
+                    local = pair * 2 + half
+                    owner = group * owners + local // per_owner
+                    outgoing[owner, local % per_owner, pl.ds(t * tile, tile), :] = joined[
+                        half
+                    ].astype(jnp.bfloat16)
+            if first and t == 0:
+                open_links()
+            if t < early:
+                for j in range(owners):
+                    send_block(group * owners + j, t)
+            if first and t == 0:
+                send_queries()
+        for j in range(owners):
+            read_own(group * owners + j)
+
+    project(0, True)
+    send_gates()
+
+    def later(step, carry):
+        project(step, False)
         return carry
 
-    lax.fori_loop(0, n, read_own, 0)
+    lax.fori_loop(1, groups, later, 0)
 
     if early < tiles:
-        @pl.loop(0, n)
-        def _(k):
-            owner = partner(k, me, n)
-            for t in range(early, tiles):
-                send_block(owner, t)
+        @pl.when(core == 0)
+        def _():
+            @pl.loop(0, n)
+            def _(k):
+                for t in range(early, tiles):
+                    send_block(partner(k, me, n), t)
 
     @pl.loop(0, n - 1)
     def _(k):
         source = partner(k, me, n)
         gate_copy(source).wait_send()
+        query_copy(source).wait_send()
         pltpu.make_async_copy(gate_in.at[source], gate_in.at[source], gate_recv.at[source]).wait()
 
     for source in range(n):
@@ -265,7 +270,7 @@
         return jnp.where(lane < head // 2, joint, both)
 
     def gather(k, carry):
-        source = partner(k, me, n)
+        source = partner(n - 2 - k, me, n)
         part_copy(source).wait_send()
         pltpu.make_async_copy(part_in.at[source], part_in.at[source], part_recv.at[source]).wait()
         return merge(carry, part_in[source])
@@ -284,34 +289,117 @@
     answer = joint / joint[:, at:at + 1]
     read[...] = pltpu.roll(answer, head, 1)[:, :head].astype(jnp.bfloat16)
 
-    for t in range(tiles):
+    def settle(t):
         block_own(t).wait()
 
         @pl.loop(0, n - 1)
-        def _(k, t=t):
+        def _(k):
             source = partner(n - 2 - k, me, n)
             block_copy(source, t).wait_send()
             pltpu.make_async_copy(
                 kv.at[:, pl.ds(t * tile, tile), :], kv.at[:, pl.ds(t * tile, tile), :], recv_sem.at[source, t]
             ).wait()
 
-
-def finish_kernel(pieces, kv, gates, answer, kv_out, gate_out, read, sem):
-    heads, length = kv.shape[0], kv.shape[1]
-    part = length // pieces
-    copies = [
-        pltpu.make_async_copy(
-            kv.at[h, pl.ds(p * part, part), :], kv_out.at[h, pl.ds(p * part, part), :], sem.at[h * pieces + p]
-        )
-        for p in range(pieces)
-        for h in range(heads)
+    for t in range(early):
+        settle(t)
+    if early < tiles:
+        @pl.when(core == 0)
+        def _():
+            for t in range(early, tiles):
+                settle(t)
+
+
+def rest_kernel(
+    n, first_row,
+    outgoing, after,
+    late,
+    send_sem, recv_sem,
+):
+    me = lax.axis_index("sp")
+    size = outgoing.shape[2] - first_row
+    held = pl.ds(first_row, size)
+
+    def rows_of(source):
+        return pl.ds(pl.multiple_of(source * size, size), size)
+
+    def block_copy(owner):
+        return pltpu.make_async_remote_copy(
+            src_ref=outgoing.at[owner, :, held, :], dst_ref=late.at[:, rows_of(me), :],
+            send_sem=send_sem.at[owner], recv_sem=recv_sem.at[me],
+            device_id={"sp": owner}, device_id_type=MESH,
+        )
+
+    @pl.when(lax.axis_index("tp") == 1)
+    def _():
+        barrier = pltpu.get_barrier_semaphore()
+
+        @pl.loop(1, n)
+        def _(k):
+            pl.semaphore_signal(
+                barrier, inc=1, device_id={"sp": lax.rem(me + k, n)}, device_id_type=MESH
+            )
+
+        pl.semaphore_wait(barrier, n - 1)
+
+        @pl.loop(0, n - 1)
+        def _(k):
+            block_copy(partner(k, me, n)).start()
+
+        late[:, rows_of(me), :] = outgoing[me, :, held, :]
+
+        @pl.loop(0, n - 1)
+        def _(k):
+            source = partner(n - 2 - k, me, n)
+            block_copy(source).wait_send()
+            pltpu.make_async_copy(
+                outgoing.at[0, :, held, :], late.at[:, rows_of(source), :], recv_sem.at[source]
+            ).wait()
+
+
+def finish_kernel(n, first_row, kv, gates, answer, kv_out, gate_out, read, sem):
+    count = kv.shape[1] // n
+
+    def part(source, start, size, at):
+        span = pl.ds(source * count + start, size)
+        return pltpu.make_async_copy(kv.at[:, span, :], kv_out.at[:, span, :], sem.at[at])
+
+    small = [
+        pltpu.make_async_copy(gates, gate_out, sem.at[2 * n]),
+        pltpu.make_async_copy(answer, read, sem.at[2 * n + 1]),
     ]
-    copies.append(pltpu.make_async_copy(gates, gate_out, sem.at[heads * pieces]))
-    copies.append(pltpu.make_async_copy(answer, read, sem.at[heads * pieces + 1]))
-    for copy in copies:
+    early = [part(source, 0, first_row, source) for source in range(n)]
+    for copy in early + small:
         copy.start()
-    for copy in copies:
+    if first_row < count:
+        @pl.when(lax.axis_index("tp") == 0)
+        def _():
+            late = [part(source, first_row, count - first_row, n + source) for source in range(n)]
+            for copy in late:
+                copy.start()
+            for copy in late:
+                copy.wait()
+    for copy in early + small:
         copy.wait()
+
+
+def last_kernel(n, first_row, late, kv, kv_out, sem):
+    count = kv_out.shape[1] // n
+    size = count - first_row
+
+    @pl.when(lax.axis_index("tp") == 1)
+    def _():
+        copies = [
+            pltpu.make_async_copy(
+                late.at[:, pl.ds(source * size, size), :],
+                kv_out.at[:, pl.ds(source * count + first_row, size), :],
+                sem.at[source],
+            )
+            for source in range(n)
+        ]
+        for copy in copies:
+            copy.start()
+        for copy in copies:
+            copy.wait()
 
 
 def on_device(n, tokens, key_weight, value_weight, cum_gate, query):
@@ -323,21 +411,22 @@
     groups = heads * head // columns
     tiles = count // tile
     any_space = pl.BlockSpec(memory_space=pl.ANY)
+    outside = pl.BlockSpec(memory_space=pltpu.HBM)
     vmem = pl.BlockSpec(memory_space=pltpu.VMEM)
-    kv, gates, answer = pl.pallas_call(
+    kv, outgoing, gates, answer = pl.pallas_call(
         functools.partial(exchange_kernel, n, per_owner, tile, head),
         name="exchange",
         out_shape=(
             pltpu.VMEM((per_owner, n * count, 2 * head), jnp.bfloat16),
+            pltpu.VMEM((n, per_owner, count, 2 * head), jnp.bfloat16),
             pltpu.VMEM((per_owner, n * count), jnp.float32),
             pltpu.VMEM((per_owner, head), jnp.bfloat16),
         ),
-        in_specs=[any_space] * 5,
-        out_specs=(vmem, vmem, vmem),
+        in_specs=[outside] * 5,
+        out_specs=(vmem, vmem, vmem, vmem),
         scratch_shapes=[
             pltpu.VMEM((count, width), jnp.bfloat16),
             pltpu.VMEM((groups, 2, width, columns), jnp.bfloat16),
-            pltpu.VMEM((n, per_owner, count, 2 * head), jnp.bfloat16),
             pltpu.VMEM((n, per_owner, 1, count), jnp.float32),
             pltpu.VMEM((n, per_owner, count), jnp.bfloat16),
             pltpu.VMEM((n, per_owner, count), jnp.bfloat16),
@@ -361,7 +450,7 @@
             pltpu.SemaphoreType.DMA((2,)),
         ],
         compiler_params=pltpu.CompilerParams(
-            collective_id=0, has_side_effects=True, vmem_limit_bytes=56 * 1024 * 1024
+            collective_id=0, has_side_effects=True, vmem_limit_bytes=48 * 1024 * 1024
         ),
     )(
         tokens.reshape(count, width),
@@ -370,20 +459,43 @@
         cum_gate.reshape(n, per_owner, 1, count),
         query.reshape(per_owner, head),
     )
-    pieces = 4 if n % 4 == 0 else 1
+    first_row = max(tiles - 1, 1) * tile
+    whole = jax.ShapeDtypeStruct((per_owner, n * count, 2 * head), jnp.bfloat16)
     kv_out, gate_out, read = pl.pallas_call(
-        functools.partial(finish_kernel, pieces),
+        functools.partial(finish_kernel, n, first_row),
         name="finish",
         out_shape=(
-            jax.ShapeDtypeStruct((per_owner, n * count, 2 * head), jnp.bfloat16),
+            whole,
             jax.ShapeDtypeStruct((per_owner, n * count), jnp.float32),
             jax.ShapeDtypeStruct((per_owner, head), jnp.bfloat16),
         ),
         in_specs=[vmem, vmem, vmem],
         out_specs=(any_space, any_space, any_space),
-        scratch_shapes=[pltpu.SemaphoreType.DMA((per_owner * pieces + 2,))],
+        scratch_shapes=[pltpu.SemaphoreType.DMA((2 * n + 2,))],
         compiler_params=pltpu.CompilerParams(vmem_limit_bytes=16 * 1024 * 1024),
     )(kv, gates, answer)
+    if first_row < count:
+        late = pl.pallas_call(
+            functools.partial(rest_kernel, n, first_row),
+            name="rest",
+            out_shape=pltpu.VMEM((per_owner, n * (count - first_row), 2 * head), jnp.bfloat16),
+            in_specs=[vmem, outside],
+            out_specs=vmem,
+            scratch_shapes=[pltpu.SemaphoreType.DMA((n,)), pltpu.SemaphoreType.DMA((n,))],
+            compiler_params=pltpu.CompilerParams(
+                collective_id=1, has_side_effects=True, vmem_limit_bytes=48 * 1024 * 1024
+            ),
+        )(outgoing, read)
+        kv_out = pl.pallas_call(
+            functools.partial(last_kernel, n, first_row),
+            name="last",
+            out_shape=whole,
+            in_specs=[vmem, any_space],
+            out_specs=any_space,
+            input_output_aliases={1: 0},
+            scratch_shapes=[pltpu.SemaphoreType.DMA((n,))],
+            compiler_params=pltpu.CompilerParams(vmem_limit_bytes=16 * 1024 * 1024),
+        )(late, kv_out)
     return kv_out[None], gate_out[None], read[None]
 
 

time: 149 us -> 148 us (level)
  Pallas kernels: 148 us -> 145 us
  local copies, waits for them, and re-layouts: 0 us -> 2.39 us
    pallas_call x1, Pallas kernels: 145 us -> 112 us  [on_device(): pl.pallas_call(functools.partial(exchange_kernel, n, per_owner, tile, hea...]
    pallas_call x1 -> x3, Pallas kernels: 2.81 us -> 32.3 us  [the longest x1 28.8 us: on_device(): pl.pallas_call(functools.partial(rest_kernel, n, first_row), name='rest',...]
    unnamed x0 -> x4, local copies, waits for them, and re-layouts: none -> 2.39 us
where the time goes in v2:
time: 148 us
  Pallas kernels  145 us (98%)
  local copies, waits for them, and re-layouts  2.39 us (2%)
    pallas_call x1, Pallas kernels, on_device(): pl.pallas_call(functools.partial(exchange_kernel, n, per_owner, tile, hea...  112 us
    pallas_call x1, Pallas kernels, on_device(): pl.pallas_call(functools.partial(rest_kernel, n, first_row), name='rest',...  28.8 us

profile of v2, /device:TPU:11, one launch (start us, length us, event | category | flops | bytes accessed | tf_op | source)
XLA Modules:
  0.0 147.8 jit_solution(15143720354024490493)
XLA Ops:
  0.6 112.4 %exchange.1 = (bf16[4,6144,128]{2,1,0:T(8,128)(2,1)S(1)}, bf16[8,4,768,128]{3,2,1,0:T(8,128)(2,1)S(1)}, f32[4,6144]{1,0:T(4,128)S(1)}, bf16[4,64]{1,0:T(4,128)(2,1)S(1)}) custom-call(bf16[768,2048]{1,0:T(8,128)(2,1)} %bitcast.8, bf16[2048,2048]{1,0:T(8,128)(2,1)} %key_weight.1, bf16[2048,2048]{1,0:T(8,128)(2,1)} %value_weight.1, f32[8,4,1,768]{3,2,1,0:T(1,128)} %bitcast.9, ...), custom_call_target="tpu_custom_call" | custom-call | tf_op jit(solution)/shard_map/exchange/pallas_call | solution.py:416
  113.0 0.0 copy-start
  113.0 2.2 %finish.1 = (bf16[4,6144,128]{2,1,0:T(8,128)(2,1)}, f32[4,6144]{1,0:T(4,128)}, bf16[4,64]{1,0:T(4,128)(2,1)}) custom-call(bf16[4,6144,128]{2,1,0:T(8,128)(2,1)S(1)} %get-tuple-element.11.kv, f32[4,6144]{1,0:T(4,128)S(1)} %get-tuple-element.12.gates, bf16[4,64]{1,0:T(4,128)(2,1)S(1)} %get-tuple-element.13.answer), custom_call_target="tpu_custom_call" | custom-call | tf_op jit(solution)/shard_map/finish/pallas_call | solution.py:464
  115.2 1.7 %copy-done = bf16[8,4,768,128]{3,2,1,0:T(8,128)(2,1)} copy-done((bf16[8,4,768,128]{3,2,1,0:T(8,128)(2,1)}, bf16[8,4,768,128]{3,2,1,0:T(8,128)(2,1)S(1)}, u32[]{:S(2)}) %copy-start) | copy-done | bytes 6291480
  117.0 0.0 copy-start.1
  117.0 0.7 copy-done.1
  117.6 28.8 %rest.1.late = bf16[4,2048,128]{2,1,0:T(8,128)(2,1)S(1)} custom-call(bf16[8,4,768,128]{3,2,1,0:T(8,128)(2,1)} %copy-done, bf16[4,64]{1,0:T(4,128)(2,1)S(1)} %copy-done.1), custom_call_target="tpu_custom_call" | custom-call | tf_op jit(solution)/shard_map/rest/pallas_call | solution.py:478
  146.4 1.4 last.1
Async XLA Ops:
  113.0 3.9 %copy-start = (bf16[8,4,768,128]{3,2,1,0:T(8,128)(2,1)}, bf16[8,4,768,128]{3,2,1,0:T(8,128)(2,1)S(1)}, u32[]{:S(2)}) copy-start(bf16[8,4,768,128]{3,2,1,0:T(8,128)(2,1)S(1)} %get-tuple-element.10.outgoing) | copy-start | bytes 18874372
  117.0 0.7 copy-start.1

commit v3 on v2

--- a/solution.py
+++ b/solution.py
@@ -356,7 +356,7 @@
             ).wait()
 
 
-def finish_kernel(n, first_row, kv, gates, answer, kv_out, gate_out, read, sem):
+def finish_kernel(n, first_row, kv, gates, answer, kv_out, gate_out, read, after, sem):
     count = kv.shape[1] // n
 
     def part(source, start, size, at):
@@ -370,6 +370,7 @@
     early = [part(source, 0, first_row, source) for source in range(n)]
     for copy in early + small:
         copy.start()
+    after[...] = jnp.zeros_like(after)
     if first_row < count:
         @pl.when(lax.axis_index("tp") == 0)
         def _():
@@ -461,16 +462,17 @@
     )
     first_row = max(tiles - 1, 1) * tile
     whole = jax.ShapeDtypeStruct((per_owner, n * count, 2 * head), jnp.bfloat16)
-    kv_out, gate_out, read = pl.pallas_call(
+    kv_out, gate_out, read, after = pl.pallas_call(
         functools.partial(finish_kernel, n, first_row),
         name="finish",
         out_shape=(
             whole,
             jax.ShapeDtypeStruct((per_owner, n * count), jnp.float32),
             jax.ShapeDtypeStruct((per_owner, head), jnp.bfloat16),
+            pltpu.VMEM((8, LANES), jnp.float32),
         ),
         in_specs=[vmem, vmem, vmem],
-        out_specs=(any_space, any_space, any_space),
+        out_specs=(any_space, any_space, any_space, vmem),
         scratch_shapes=[pltpu.SemaphoreType.DMA((2 * n + 2,))],
         compiler_params=pltpu.CompilerParams(vmem_limit_bytes=16 * 1024 * 1024),
     )(kv, gates, answer)
@@ -479,13 +481,13 @@
             functools.partial(rest_kernel, n, first_row),
             name="rest",
             out_shape=pltpu.VMEM((per_owner, n * (count - first_row), 2 * head), jnp.bfloat16),
-            in_specs=[vmem, outside],
+            in_specs=[vmem, vmem],
             out_specs=vmem,
             scratch_shapes=[pltpu.SemaphoreType.DMA((n,)), pltpu.SemaphoreType.DMA((n,))],
             compiler_params=pltpu.CompilerParams(
-                collective_id=1, has_side_effects=True, vmem_limit_bytes=48 * 1024 * 1024
+                collective_id=1, has_side_effects=True, vmem_limit_bytes=16 * 1024 * 1024
             ),
-        )(outgoing, read)
+        )(outgoing, after)
         kv_out = pl.pallas_call(
             functools.partial(last_kernel, n, first_row),
             name="last",

time: 148 us -> 145 us (0.980)
  local copies, waits for them, and re-layouts: 2.39 us -> 0 us
    unnamed x4 -> x0, local copies, waits for them, and re-layouts: 2.39 us -> none
where the time goes in v3:
time: 145 us
  Pallas kernels  144 us (99%)
    pallas_call x1, Pallas kernels, on_device(): pl.pallas_call(functools.partial(exchange_kernel, n, per_owner, tile, hea...  112 us
    pallas_call x1, Pallas kernels, on_device(): pl.pallas_call(functools.partial(rest_kernel, n, first_row), name='rest',...  28.5 us

profile of v3, /device:TPU:11, one launch (start us, length us, event | category | flops | bytes accessed | tf_op | source)
XLA Modules:
  0.0 145.1 jit_solution(15103254142659224571)
XLA Ops:
  0.6 112.4 %exchange.1 = (bf16[4,6144,128]{2,1,0:T(8,128)(2,1)S(1)}, bf16[8,4,768,128]{3,2,1,0:T(8,128)(2,1)S(1)}, f32[4,6144]{1,0:T(4,128)S(1)}, bf16[4,64]{1,0:T(4,128)(2,1)S(1)}) custom-call(bf16[768,2048]{1,0:T(8,128)(2,1)} %bitcast.7, bf16[2048,2048]{1,0:T(8,128)(2,1)} %key_weight.1, bf16[2048,2048]{1,0:T(8,128)(2,1)} %value_weight.1, f32[8,4,1,768]{3,2,1,0:T(1,128)} %bitcast.8, ...), custom_call_target="tpu_custom_call" | custom-call | tf_op jit(solution)/shard_map/exchange/pallas_call | solution.py:417
  113.0 2.2 %finish.1 = (bf16[4,6144,128]{2,1,0:T(8,128)(2,1)}, f32[4,6144]{1,0:T(4,128)}, bf16[4,64]{1,0:T(4,128)(2,1)}, f32[8,128]{1,0:T(8,128)S(1)}) custom-call(bf16[4,6144,128]{2,1,0:T(8,128)(2,1)S(1)} %get-tuple-element.12.kv, f32[4,6144]{1,0:T(4,128)S(1)} %get-tuple-element.13.gates, bf16[4,64]{1,0:T(4,128)(2,1)S(1)} %get-tuple-element.14.answer), custom_call_target="tpu_custom_call" | custom-call | tf_op jit(solution)/shard_map/finish/pallas_call | solution.py:465
  115.2 28.5 %rest.1.late = bf16[4,2048,128]{2,1,0:T(8,128)(2,1)S(1)} custom-call(bf16[8,4,768,128]{3,2,1,0:T(8,128)(2,1)S(1)} %get-tuple-element.11.outgoing, f32[8,128]{1,0:T(8,128)S(1)} %get-tuple-element.15.after), custom_call_target="tpu_custom_call" | custom-call | tf_op jit(solution)/shard_map/rest/pallas_call | solution.py:480
  143.7 1.4 last.1

commit v4 on v3

--- a/solution.py
+++ b/solution.py
@@ -24,11 +24,11 @@
 
 
 def exchange_kernel(
-    n, per_owner, tile, head,
+    n, per_owner, tile, head, ahead_rows,
     tokens, key_weight, value_weight, gates, query,
     kv, outgoing, gate_out, read,
-    rows, weights, gate_own, gate_send, gate_in, query_own, query_in, part_send, part_in, mine, theirs,
-    row_sem, weight_sem, small_sem, send_sem, recv_sem,
+    rows, weights, gate_own, gate_send, gate_in, query_own, query_in, part_send, part_in, mine, theirs, row_in, relayed,
+    row_sem, weight_sem, small_sem, send_sem, recv_sem, known_sem, ahead_sem, relay_sent, relay_recv,
     gate_sent, gate_recv, query_sent, query_recv, part_sent, part_recv, pair_sem,
 ):
     me = lax.axis_index("sp")
@@ -42,12 +42,10 @@
     groups = n // owners
 
     def group_of(step):
-        if owners == 1:
-            return partner(step, me, n, core)
-        return lax.rem(me // owners + 1 + step, groups)
+        return partner(step, me // owners, groups, core)
 
     def load_rows(t):
-        span = pl.ds(t * tile, tile)
+        span = pl.ds(t * tile, tile - ahead_rows if t == early - 1 else tile)
         return pltpu.make_async_copy(tokens.at[span, :], rows.at[span, :], row_sem.at[t])
 
     def load_weight(step, which):
@@ -59,23 +57,67 @@
 
     load_query = pltpu.make_async_copy(query, query_own, small_sem.at[0])
     load_gates = pltpu.make_async_copy(gates, gate_own, small_sem.at[1])
-    load_query.start()
+
+    layers = n // 2
+    layer = me // 2
+    near = layers // 2
+    right = layer >= near
+    inner = (layer == near - 1) | (layer == near)
+    mate = jnp.where(right, me - 2, me + 2)
+    ahead_tile = early - 1
+    ahead_at = (ahead_tile + 1) * tile - ahead_rows
+    ahead_span = pl.ds(ahead_at, ahead_rows)
+
+    def crosses(owner):
+        return (owner // 2 >= near) != right
+
+    def is_inner(owner):
+        return (owner // 2 == near - 1) | (owner // 2 == near)
+
+    barrier = pltpu.get_barrier_semaphore()
+    neighbours = 1 + (layer > 0).astype(jnp.int32) + (layer < layers - 1).astype(jnp.int32)
+
+    def tell_neighbours(sem):
+        @pl.when(layer > 0)
+        def _():
+            pl.semaphore_signal(sem, inc=1, device_id={"sp": me - 2}, device_id_type=MESH)
+
+        @pl.when(layer < layers - 1)
+        def _():
+            pl.semaphore_signal(sem, inc=1, device_id={"sp": me + 2}, device_id_type=MESH)
+
+        pl.semaphore_signal(
+            sem, inc=1, device_id={"sp": me + 1 - 2 * lax.rem(me, 2)}, device_id_type=MESH
+        )
+
+    tell_neighbours(barrier)
+    pl.semaphore_signal(barrier, inc=1, device_id={"tp": 1 - core}, device_id_type=MESH)
+    load_ahead = pltpu.make_async_copy(
+        tokens.at[ahead_span, :], rows.at[ahead_span, :], small_sem.at[2]
+    )
+    load_ahead.start()
     load_rows(0).start()
     load_weight(0, 0).start()
     load_weight(0, 1).start()
     load_gates.start()
+    load_query.start()
     for t in range(1, tiles):
         load_rows(t).start()
-
-    barrier = pltpu.get_barrier_semaphore()
-
-    @pl.loop(1, n)
-    def _(k):
-        pl.semaphore_signal(
-            barrier, inc=1, device_id={"sp": lax.rem(me + k, n)}, device_id_type=MESH
-        )
-
-    pl.semaphore_signal(barrier, inc=1, device_id={"tp": 1 - core}, device_id_type=MESH)
+    send_ahead = pltpu.make_async_remote_copy(
+        src_ref=rows.at[ahead_span, :], dst_ref=row_in,
+        send_sem=ahead_sem.at[0], recv_sem=ahead_sem.at[1],
+        device_id={"sp": mate}, device_id_type=MESH,
+    )
+    load_ahead.wait()
+    pl.semaphore_wait(barrier, neighbours + 1)
+
+    @pl.when(inner)
+    def _():
+        send_ahead.start()
+
+    tell_neighbours(known_sem.at[0])
+    pl.semaphore_wait(known_sem.at[0], neighbours)
+    tell_neighbours(known_sem.at[1])
 
     def query_copy(owner):
         return pltpu.make_async_remote_copy(
@@ -98,13 +140,25 @@
             device_id={"sp": owner}, device_id_type=MESH,
         )
 
-    def block_copy(owner, t):
+    def block_copy(owner, t, size=tile):
         return pltpu.make_async_remote_copy(
-            src_ref=outgoing.at[owner, :, pl.ds(t * tile, tile), :],
-            dst_ref=kv.at[:, pl.ds(pl.multiple_of(me * count + t * tile, tile), tile), :],
+            src_ref=outgoing.at[owner, :, pl.ds(t * tile, size), :],
+            dst_ref=kv.at[:, pl.ds(pl.multiple_of(me * count + t * tile, LANES), size), :],
             send_sem=send_sem.at[owner, t], recv_sem=recv_sem.at[me, t],
             device_id={"sp": owner}, device_id_type=MESH,
         )
+
+    def both_sizes(t, short, act):
+        if t == ahead_tile:
+            @pl.when(short)
+            def _():
+                act(tile - ahead_rows)
+
+            @pl.when(jnp.logical_not(short))
+            def _():
+                act(tile)
+        else:
+            act(tile)
 
     def block_own(t):
         return pltpu.make_async_copy(
@@ -116,7 +170,7 @@
     def send_block(owner, t):
         @pl.when(owner != me)
         def _():
-            block_copy(owner, t).start()
+            both_sizes(t, inner & crosses(owner), lambda size: block_copy(owner, t, size).start())
 
         @pl.when(owner == me)
         def _():
@@ -128,7 +182,12 @@
     low = lax.broadcasted_iota(jnp.int32, (tile, LANES), 1) < head
 
     def open_links():
-        pl.semaphore_wait(barrier, n)
+        pl.semaphore_wait(known_sem.at[1], neighbours)
+
+        @pl.loop(2, layers - 1)
+        def _(k):
+            tell_neighbours(known_sem.at[k])
+            pl.semaphore_wait(known_sem.at[k], neighbours)
 
     def send_queries():
         load_gates.wait()
@@ -192,7 +251,7 @@
         def _():
             part_copy(owner).start()
 
-    def project(step, first):
+    def project(step, first, relays=False):
         group = group_of(step)
 
         if first:
@@ -207,25 +266,32 @@
 
         load_weight(step, 0).wait()
         load_weight(step, 1).wait()
-        for t in range(tiles):
-            if first:
-                load_rows(t).wait()
-            left = rows[pl.ds(t * tile, tile), :]
+
+        def multiply(left, store):
+            size = left.shape[0]
             keys = jnp.dot(left, weights[step, 0], preferred_element_type=jnp.float32)
             values = jnp.dot(left, weights[step, 1], preferred_element_type=jnp.float32)
             for pair in range(columns // LANES):
                 span = slice(pair * LANES, (pair + 1) * LANES)
                 k, v = keys[:, span], values[:, span]
                 joined = (
-                    jnp.where(low, k, pltpu.roll(v, head, 1)),
-                    jnp.where(low, pltpu.roll(k, head, 1), v),
+                    jnp.where(low[:size], k, pltpu.roll(v, head, 1)),
+                    jnp.where(low[:size], pltpu.roll(k, head, 1), v),
                 )
                 for half in range(2):
                     local = pair * 2 + half
-                    owner = group * owners + local // per_owner
-                    outgoing[owner, local % per_owner, pl.ds(t * tile, tile), :] = joined[
-                        half
-                    ].astype(jnp.bfloat16)
+                    store(
+                        group * owners + local // per_owner, local % per_owner, joined[half].astype(jnp.bfloat16)
+                    )
+
+        for t in range(tiles):
+            if first:
+                load_rows(t).wait()
+
+            def keep(owner, h, block):
+                outgoing[owner, h, pl.ds(t * tile, tile), :] = block
+
+            multiply(rows[pl.ds(t * tile, tile), :], keep)
             if first and t == 0:
                 open_links()
             if t < early:
@@ -235,15 +301,51 @@
                 send_queries()
         for j in range(owners):
             read_own(group * owners + j)
+        if relays:
+            @pl.when(inner)
+            def _():
+                def keep(owner, h, block):
+                    relayed[owner, h] = block
+
+                multiply(row_in[...], keep)
+                for j in range(owners):
+                    owner = group * owners + j
+
+                    @pl.when(owner != me)
+                    def _():
+                        relay_copy(owner).start()
+
+                    @pl.when(owner == me)
+                    def _():
+                        kv[:, mate_rows, :] = relayed[owner]
+
+    mate_rows = pl.ds(pl.multiple_of(mate * count + ahead_at, 16), ahead_rows)
+
+    def relay_copy(owner):
+        return pltpu.make_async_remote_copy(
+            src_ref=relayed.at[owner], dst_ref=kv.at[:, mate_rows, :],
+            send_sem=relay_sent.at[owner], recv_sem=relay_recv.at[me],
+            device_id={"sp": owner}, device_id_type=MESH,
+        )
 
     project(0, True)
     send_gates()
 
-    def later(step, carry):
+    def across(step, carry):
         project(step, False)
         return carry
 
-    lax.fori_loop(1, groups, later, 0)
+    lax.fori_loop(1, groups // 2, across, 0)
+
+    @pl.when(inner)
+    def _():
+        send_ahead.wait()
+
+    def along(step, carry):
+        project(step, False, True)
+        return carry
+
+    lax.fori_loop(groups // 2, groups, along, 0)
 
     if early < tiles:
         @pl.when(core == 0)
@@ -295,10 +397,35 @@
         @pl.loop(0, n - 1)
         def _(k):
             source = partner(n - 2 - k, me, n)
-            block_copy(source, t).wait_send()
+            both_sizes(t, inner & crosses(source), lambda size: block_copy(source, t, size).wait_send())
+
+            def arrived(size):
+                span = pl.ds(t * tile, size)
+                pltpu.make_async_copy(kv.at[:, span, :], kv.at[:, span, :], recv_sem.at[source, t]).wait()
+
+            both_sizes(t, is_inner(source) & crosses(source), arrived)
+
+    first_inner = jnp.where(right, near, near - 1) * 2
+
+    @pl.loop(0, 2)
+    def _(k):
+        source = first_inner + k
+
+        @pl.when(source != me)
+        def _():
             pltpu.make_async_copy(
-                kv.at[:, pl.ds(t * tile, tile), :], kv.at[:, pl.ds(t * tile, tile), :], recv_sem.at[source, t]
+                kv.at[:, ahead_span, :], kv.at[:, ahead_span, :], relay_recv.at[source]
             ).wait()
+
+    @pl.when(inner)
+    def _():
+        @pl.loop(0, n // 2)
+        def _(k):
+            owner = jnp.where(right, n // 2, 0) + k
+
+            @pl.when(owner != me)
+            def _():
+                relay_copy(owner).wait_send()
 
     for t in range(early):
         settle(t)
@@ -411,11 +538,12 @@
     columns = max(per_owner * head, LANES)
     groups = heads * head // columns
     tiles = count // tile
+    ahead_rows = tile // 8
     any_space = pl.BlockSpec(memory_space=pl.ANY)
     outside = pl.BlockSpec(memory_space=pltpu.HBM)
     vmem = pl.BlockSpec(memory_space=pltpu.VMEM)
     kv, outgoing, gates, answer = pl.pallas_call(
-        functools.partial(exchange_kernel, n, per_owner, tile, head),
+        functools.partial(exchange_kernel, n, per_owner, tile, head, ahead_rows),
         name="exchange",
         out_shape=(
             pltpu.VMEM((per_owner, n * count, 2 * head), jnp.bfloat16),
@@ -437,11 +565,17 @@
             pltpu.VMEM((n, per_owner, LANES), jnp.float32),
             pltpu.VMEM((per_owner, LANES), jnp.float32),
             pltpu.VMEM((per_owner, LANES), jnp.float32),
+            pltpu.VMEM((ahead_rows, width), jnp.bfloat16),
+            pltpu.VMEM((n, per_owner, ahead_rows, 2 * head), jnp.bfloat16),
             pltpu.SemaphoreType.DMA((tiles,)),
             pltpu.SemaphoreType.DMA((groups, 2)),
-            pltpu.SemaphoreType.DMA((2,)),
+            pltpu.SemaphoreType.DMA((3,)),
             pltpu.SemaphoreType.DMA((n, tiles)),
             pltpu.SemaphoreType.DMA((n, tiles)),
+            pltpu.SemaphoreType.REGULAR((n // 2,)),
+            pltpu.SemaphoreType.DMA((2,)),
+            pltpu.SemaphoreType.DMA((n,)),
+            pltpu.SemaphoreType.DMA((n,)),
             pltpu.SemaphoreType.DMA((n,)),
             pltpu.SemaphoreType.DMA((n,)),
             pltpu.SemaphoreType.DMA((n,)),

time: 145 us -> 144 us (level)
  no operation moved by 1% of the time
where the time goes in v4:
time: 144 us
  Pallas kernels  143 us (99%)
    pallas_call x1, Pallas kernels, on_device(): pl.pallas_call(functools.partial(exchange_kernel, n, per_owner, tile, hea...  111 us
    pallas_call x1, Pallas kernels, on_device(): pl.pallas_call(functools.partial(rest_kernel, n, first_row), name='rest',...  28.1 us

profile of v4, /device:TPU:11, one launch (start us, length us, event | category | flops | bytes accessed | tf_op | source)
XLA Modules:
  0.0 143.6 jit_solution(13972493138317439593)
XLA Ops:
  0.6 111.2 %exchange.1 = (bf16[4,6144,128]{2,1,0:T(8,128)(2,1)S(1)}, bf16[8,4,768,128]{3,2,1,0:T(8,128)(2,1)S(1)}, f32[4,6144]{1,0:T(4,128)S(1)}, bf16[4,64]{1,0:T(4,128)(2,1)S(1)}) custom-call(bf16[768,2048]{1,0:T(8,128)(2,1)} %bitcast.7, bf16[2048,2048]{1,0:T(8,128)(2,1)} %key_weight.1, bf16[2048,2048]{1,0:T(8,128)(2,1)} %value_weight.1, f32[8,4,1,768]{3,2,1,0:T(1,128)} %bitcast.8, ...), custom_call_target="tpu_custom_call" | custom-call | tf_op jit(solution)/shard_map/exchange/pallas_call | solution.py:545
  111.9 2.2 %finish.1 = (bf16[4,6144,128]{2,1,0:T(8,128)(2,1)}, f32[4,6144]{1,0:T(4,128)}, bf16[4,64]{1,0:T(4,128)(2,1)}, f32[8,128]{1,0:T(8,128)S(1)}) custom-call(bf16[4,6144,128]{2,1,0:T(8,128)(2,1)S(1)} %get-tuple-element.12.kv, f32[4,6144]{1,0:T(4,128)S(1)} %get-tuple-element.13.gates, bf16[4,64]{1,0:T(4,128)(2,1)S(1)} %get-tuple-element.14.answer), custom_call_target="tpu_custom_call" | custom-call | tf_op jit(solution)/shard_map/finish/pallas_call | solution.py:599
  114.1 28.1 %rest.1.late = bf16[4,2048,128]{2,1,0:T(8,128)(2,1)S(1)} custom-call(bf16[8,4,768,128]{3,2,1,0:T(8,128)(2,1)S(1)} %get-tuple-element.11.outgoing, f32[8,128]{1,0:T(8,128)S(1)} %get-tuple-element.15.after), custom_call_target="tpu_custom_call" | custom-call | tf_op jit(solution)/shard_map/rest/pallas_call | solution.py:614
  142.2 1.4 last.1

commit v5 on v4

--- a/solution.py
+++ b/solution.py
@@ -90,8 +90,30 @@
             sem, inc=1, device_id={"sp": me + 1 - 2 * lax.rem(me, 2)}, device_id_type=MESH
         )
 
-    tell_neighbours(barrier)
-    pl.semaphore_signal(barrier, inc=1, device_id={"tp": 1 - core}, device_id_type=MESH)
+    side = lax.rem(me, 2)
+    outward = jnp.where(right, me + 2, me - 2)
+    inward = jnp.where(right, me - 2, me + 2)
+    has_outward = jnp.logical_not((layer == 0) | (layer == layers - 1))
+
+    def tell(sem, to):
+        pl.semaphore_signal(sem, inc=1, device_id=to, device_id_type=MESH)
+
+    @pl.when(inner)
+    def _():
+        tell(barrier, {"sp": mate})
+
+    @pl.when(side == 0)
+    def _():
+        tell(barrier, {"sp": me + 1})
+
+    @pl.when(core == 0)
+    def _():
+        tell(barrier, {"tp": 1 - core})
+
+    @pl.when(has_outward)
+    def _():
+        tell(barrier, {"sp": outward})
+
     load_ahead = pltpu.make_async_copy(
         tokens.at[ahead_span, :], rows.at[ahead_span, :], small_sem.at[2]
     )
@@ -109,15 +131,33 @@
         device_id={"sp": mate}, device_id_type=MESH,
     )
     load_ahead.wait()
-    pl.semaphore_wait(barrier, neighbours + 1)
+    pl.semaphore_wait(barrier, 1 + side + core)
 
     @pl.when(inner)
     def _():
         send_ahead.start()
 
-    tell_neighbours(known_sem.at[0])
-    pl.semaphore_wait(known_sem.at[0], neighbours)
+    @pl.when(jnp.logical_not(inner))
+    def _():
+        tell(known_sem.at[0], {"sp": inward})
+
+    @pl.when(side == 1)
+    def _():
+        tell(known_sem.at[0], {"sp": me - 1})
+
+    @pl.when(core == 1)
+    def _():
+        tell(known_sem.at[0], {"tp": 1 - core})
+
+    replies = has_outward.astype(jnp.int32) + 2 - side - core
+
+    @pl.when(replies > 0)
+    def _():
+        pl.semaphore_wait(known_sem.at[0], replies)
+
     tell_neighbours(known_sem.at[1])
+    pl.semaphore_wait(known_sem.at[1], neighbours)
+    tell_neighbours(known_sem.at[2])
 
     def query_copy(owner):
         return pltpu.make_async_remote_copy(
@@ -181,20 +221,19 @@
 
     low = lax.broadcasted_iota(jnp.int32, (tile, LANES), 1) < head
 
-    def open_links():
-        pl.semaphore_wait(known_sem.at[1], neighbours)
-
-        @pl.loop(2, layers - 1)
-        def _(k):
-            tell_neighbours(known_sem.at[k])
-            pl.semaphore_wait(known_sem.at[k], neighbours)
+    def open_links(first_round, last_round):
+        for at in range(first_round - 1, last_round):
+            pl.semaphore_wait(known_sem.at[at], neighbours)
+            if at + 1 < layers:
+                tell_neighbours(known_sem.at[at + 1])
 
     def send_queries():
         load_gates.wait()
         load_query.wait()
-        query_in[me] = jnp.concatenate(
+        wide = jnp.concatenate(
             [query_own[...].astype(jnp.float32), jnp.zeros((per_owner, LANES - head), jnp.float32)], axis=1
         ) * (head ** -0.5)
+        query_in[me] = wide.astype(jnp.bfloat16)
 
         @pl.loop(0, n - 1)
         def _(k):
@@ -218,7 +257,7 @@
         def _():
             pltpu.make_async_copy(query_in.at[owner], query_in.at[owner], query_recv.at[owner]).wait()
 
-        asked = query_in[owner]
+        asked = query_in[owner].astype(jnp.float32)
         queries = [
             jnp.where(head_row == h, asked, 0.0).astype(jnp.bfloat16) for h in range(per_owner)
         ]
@@ -293,8 +332,20 @@
 
             multiply(rows[pl.ds(t * tile, tile), :], keep)
             if first and t == 0:
-                open_links()
-            if t < early:
+                open_links(3, near + 1)
+
+                @pl.when(inner)
+                def _():
+                    for j in range(owners):
+                        send_block(group * owners + j, t)
+
+                open_links(near + 2, layers)
+
+                @pl.when(jnp.logical_not(inner))
+                def _():
+                    for j in range(owners):
+                        send_block(group * owners + j, t)
+            elif t < early:
                 for j in range(owners):
                     send_block(group * owners + j, t)
             if first and t == 0:
@@ -560,7 +611,7 @@
             pltpu.VMEM((n, per_owner, count), jnp.bfloat16),
             pltpu.VMEM((n, per_owner, count), jnp.bfloat16),
             pltpu.VMEM((per_owner, head), jnp.bfloat16),
-            pltpu.VMEM((n, per_owner, LANES), jnp.float32),
+            pltpu.VMEM((n, per_owner, LANES), jnp.bfloat16),
             pltpu.VMEM((n, per_owner, LANES), jnp.float32),
             pltpu.VMEM((n, per_owner, LANES), jnp.float32),
             pltpu.VMEM((per_owner, LANES), jnp.float32),

time: 144 us -> 143 us (level)
  no operation moved by 1% of the time
where the time goes in v5:
time: 143 us
  Pallas kernels  142 us (99%)
    pallas_call x1, Pallas kernels, on_device(): pl.pallas_call(functools.partial(exchange_kernel, n, per_owner, tile, hea...  110 us
    pallas_call x1, Pallas kernels, on_device(): pl.pallas_call(functools.partial(rest_kernel, n, first_row), name='rest',...  28.1 us

profile of v5, /device:TPU:11, one launch (start us, length us, event | category | flops | bytes accessed | tf_op | source)
XLA Modules:
  0.0 142.8 jit_solution(9409104447043565997)
XLA Ops:
  0.6 110.5 %exchange.1 = (bf16[4,6144,128]{2,1,0:T(8,128)(2,1)S(1)}, bf16[8,4,768,128]{3,2,1,0:T(8,128)(2,1)S(1)}, f32[4,6144]{1,0:T(4,128)S(1)}, bf16[4,64]{1,0:T(4,128)(2,1)S(1)}) custom-call(bf16[768,2048]{1,0:T(8,128)(2,1)} %bitcast.7, bf16[2048,2048]{1,0:T(8,128)(2,1)} %key_weight.1, bf16[2048,2048]{1,0:T(8,128)(2,1)} %value_weight.1, f32[8,4,1,768]{3,2,1,0:T(1,128)} %bitcast.8, ...), custom_call_target="tpu_custom_call" | custom-call | tf_op jit(solution)/shard_map/exchange/pallas_call | solution.py:596
  111.1 2.2 %finish.1 = (bf16[4,6144,128]{2,1,0:T(8,128)(2,1)}, f32[4,6144]{1,0:T(4,128)}, bf16[4,64]{1,0:T(4,128)(2,1)}, f32[8,128]{1,0:T(8,128)S(1)}) custom-call(bf16[4,6144,128]{2,1,0:T(8,128)(2,1)S(1)} %get-tuple-element.12.kv, f32[4,6144]{1,0:T(4,128)S(1)} %get-tuple-element.13.gates, bf16[4,64]{1,0:T(4,128)(2,1)S(1)} %get-tuple-element.14.answer), custom_call_target="tpu_custom_call" | custom-call | tf_op jit(solution)/shard_map/finish/pallas_call | solution.py:650
  113.3 28.1 %rest.1.late = bf16[4,2048,128]{2,1,0:T(8,128)(2,1)S(1)} custom-call(bf16[8,4,768,128]{3,2,1,0:T(8,128)(2,1)S(1)} %get-tuple-element.11.outgoing, f32[8,128]{1,0:T(8,128)S(1)} %get-tuple-element.15.after), custom_call_target="tpu_custom_call" | custom-call | tf_op jit(solution)/shard_map/rest/pallas_call | solution.py:665
  141.4 1.4 last.1

commit v6 on v5

--- a/solution.py
+++ b/solution.py
@@ -521,7 +521,7 @@
 
         @pl.loop(0, n - 1)
         def _(k):
-            block_copy(partner(k, me, n)).start()
+            block_copy(partner(k, me, n, 1)).start()
 
         late[:, rows_of(me), :] = outgoing[me, :, held, :]
 

time: 143 us -> 143 us (level)
  no operation moved by 1% of the time
where the time goes in v6:
time: 143 us; the launch traced here: 142 us
  Pallas kernels  142 us (99%)
    pallas_call x1, Pallas kernels, on_device(): pl.pallas_call(functools.partial(exchange_kernel, n, per_owner, tile, hea...  110 us
    pallas_call x1, Pallas kernels, on_device(): pl.pallas_call(functools.partial(rest_kernel, n, first_row), name='rest',...  27.7 us

profile of v6, /device:TPU:11, one launch (start us, length us, event | category | flops | bytes accessed | tf_op | source)
XLA Modules:
  0.0 142.4 jit_solution(814324360378268668)
XLA Ops:
  0.6 110.5 %exchange.1 = (bf16[4,6144,128]{2,1,0:T(8,128)(2,1)S(1)}, bf16[8,4,768,128]{3,2,1,0:T(8,128)(2,1)S(1)}, f32[4,6144]{1,0:T(4,128)S(1)}, bf16[4,64]{1,0:T(4,128)(2,1)S(1)}) custom-call(bf16[768,2048]{1,0:T(8,128)(2,1)} %bitcast.7, bf16[2048,2048]{1,0:T(8,128)(2,1)} %key_weight.1, bf16[2048,2048]{1,0:T(8,128)(2,1)} %value_weight.1, f32[8,4,1,768]{3,2,1,0:T(1,128)} %bitcast.8, ...), custom_call_target="tpu_custom_call" | custom-call | tf_op jit(solution)/shard_map/exchange/pallas_call | solution.py:596
  111.1 2.2 %finish.1 = (bf16[4,6144,128]{2,1,0:T(8,128)(2,1)}, f32[4,6144]{1,0:T(4,128)}, bf16[4,64]{1,0:T(4,128)(2,1)}, f32[8,128]{1,0:T(8,128)S(1)}) custom-call(bf16[4,6144,128]{2,1,0:T(8,128)(2,1)S(1)} %get-tuple-element.12.kv, f32[4,6144]{1,0:T(4,128)S(1)} %get-tuple-element.13.gates, bf16[4,64]{1,0:T(4,128)(2,1)S(1)} %get-tuple-element.14.answer), custom_call_target="tpu_custom_call" | custom-call | tf_op jit(solution)/shard_map/finish/pallas_call | solution.py:650
  113.3 27.7 %rest.1.late = bf16[4,2048,128]{2,1,0:T(8,128)(2,1)S(1)} custom-call(bf16[8,4,768,128]{3,2,1,0:T(8,128)(2,1)S(1)} %get-tuple-element.11.outgoing, f32[8,128]{1,0:T(8,128)S(1)} %get-tuple-element.15.after), custom_call_target="tpu_custom_call" | custom-call | tf_op jit(solution)/shard_map/rest/pallas_call | solution.py:665
  141.0 1.4 last.1

commit v7 on v6

--- a/solution.py
+++ b/solution.py
@@ -283,8 +283,12 @@
                 picked = jnp.where(tile_row == h, probs, 0.0).astype(jnp.bfloat16)
                 weighted = weighted + jnp.dot(picked, blocks[h], preferred_element_type=jnp.float32)
             top = new_top
-        packed = jnp.where(lane < head // 2, top, jnp.where(lane < head, total, weighted))
-        part_send[owner] = packed
+        level = top + jnp.log(total)
+        first = level.astype(jnp.bfloat16).astype(jnp.float32)
+        second = (level - first).astype(jnp.bfloat16).astype(jnp.float32)
+        third = level - first - second
+        words = jnp.where(lane == 0, first, jnp.where(lane == 1, second, third))
+        part_send[owner] = jnp.where(lane < head, words, weighted / total).astype(jnp.bfloat16)
 
         @pl.when(owner != me)
         def _():
@@ -422,13 +426,18 @@
         both = one * jnp.exp(top_one - joint) + two * jnp.exp(top_two - joint)
         return jnp.where(lane < head // 2, joint, both)
 
+    def unpack(part):
+        words = part.astype(jnp.float32)
+        level = words[:, 0:1] + words[:, 1:2] + words[:, 2:3]
+        return jnp.where(lane < head // 2, level, jnp.where(lane < head, 1.0, words))
+
     def gather(k, carry):
         source = partner(n - 2 - k, me, n)
         part_copy(source).wait_send()
         pltpu.make_async_copy(part_in.at[source], part_in.at[source], part_recv.at[source]).wait()
-        return merge(carry, part_in[source])
-
-    packed = lax.fori_loop(0, n - 1, gather, part_send[me])
+        return merge(carry, unpack(part_in[source]))
+
+    packed = lax.fori_loop(0, n - 1, gather, unpack(part_send[me]))
     mine[...] = packed
     swap = pltpu.make_async_remote_copy(
         src_ref=mine, dst_ref=theirs, send_sem=pair_sem.at[0], recv_sem=pair_sem.at[1],
@@ -612,8 +621,8 @@
             pltpu.VMEM((n, per_owner, count), jnp.bfloat16),
             pltpu.VMEM((per_owner, head), jnp.bfloat16),
             pltpu.VMEM((n, per_owner, LANES), jnp.bfloat16),
-            pltpu.VMEM((n, per_owner, LANES), jnp.float32),
-            pltpu.VMEM((n, per_owner, LANES), jnp.float32),
+            pltpu.VMEM((n, per_owner, LANES), jnp.bfloat16),
+            pltpu.VMEM((n, per_owner, LANES), jnp.bfloat16),
             pltpu.VMEM((per_owner, LANES), jnp.float32),
             pltpu.VMEM((per_owner, LANES), jnp.float32),
             pltpu.VMEM((ahead_rows, width), jnp.bfloat16),

time: 143 us -> 142 us (level)
  no operation moved by 1% of the time
where the time goes in v7:
time: 142 us
  Pallas kernels  142 us (100%)
    pallas_call x1, Pallas kernels, on_device(): pl.pallas_call(functools.partial(exchange_kernel, n, per_owner, tile, hea...  111 us
    pallas_call x1, Pallas kernels, on_device(): pl.pallas_call(functools.partial(rest_kernel, n, first_row), name='rest',...  27.1 us

profile of v7, /device:TPU:11, one launch (start us, length us, event | category | flops | bytes accessed | tf_op | source)
XLA Modules:
  0.0 142.2 jit_solution(4604182388595034096)
XLA Ops:
  0.6 110.9 %exchange.1 = (bf16[4,6144,128]{2,1,0:T(8,128)(2,1)S(1)}, bf16[8,4,768,128]{3,2,1,0:T(8,128)(2,1)S(1)}, f32[4,6144]{1,0:T(4,128)S(1)}, bf16[4,64]{1,0:T(4,128)(2,1)S(1)}) custom-call(bf16[768,2048]{1,0:T(8,128)(2,1)} %bitcast.7, bf16[2048,2048]{1,0:T(8,128)(2,1)} %key_weight.1, bf16[2048,2048]{1,0:T(8,128)(2,1)} %value_weight.1, f32[8,4,1,768]{3,2,1,0:T(1,128)} %bitcast.8, ...), custom_call_target="tpu_custom_call" | custom-call | tf_op jit(solution)/shard_map/exchange/pallas_call | solution.py:605
  111.5 2.2 %finish.1 = (bf16[4,6144,128]{2,1,0:T(8,128)(2,1)}, f32[4,6144]{1,0:T(4,128)}, bf16[4,64]{1,0:T(4,128)(2,1)}, f32[8,128]{1,0:T(8,128)S(1)}) custom-call(bf16[4,6144,128]{2,1,0:T(8,128)(2,1)S(1)} %get-tuple-element.12.kv, f32[4,6144]{1,0:T(4,128)S(1)} %get-tuple-element.13.gates, bf16[4,64]{1,0:T(4,128)(2,1)S(1)} %get-tuple-element.14.answer), custom_call_target="tpu_custom_call" | custom-call | tf_op jit(solution)/shard_map/finish/pallas_call | solution.py:659
  113.7 27.1 %rest.1.late = bf16[4,2048,128]{2,1,0:T(8,128)(2,1)S(1)} custom-call(bf16[8,4,768,128]{3,2,1,0:T(8,128)(2,1)S(1)} %get-tuple-element.11.outgoing, f32[8,128]{1,0:T(8,128)S(1)} %get-tuple-element.15.after), custom_call_target="tpu_custom_call" | custom-call | tf_op jit(solution)/shard_map/rest/pallas_call | solution.py:674
  140.8 1.4 last.1

commit v8 on v7

--- a/solution.py
+++ b/solution.py
@@ -230,10 +230,7 @@
     def send_queries():
         load_gates.wait()
         load_query.wait()
-        wide = jnp.concatenate(
-            [query_own[...].astype(jnp.float32), jnp.zeros((per_owner, LANES - head), jnp.float32)], axis=1
-        ) * (head ** -0.5)
-        query_in[me] = wide.astype(jnp.bfloat16)
+        query_in[me] = (query_own[...].astype(jnp.float32) * (head ** -0.5)).astype(jnp.bfloat16)
 
         @pl.loop(0, n - 1)
         def _(k):
@@ -257,7 +254,9 @@
         def _():
             pltpu.make_async_copy(query_in.at[owner], query_in.at[owner], query_recv.at[owner]).wait()
 
-        asked = query_in[owner].astype(jnp.float32)
+        asked = jnp.concatenate(
+            [query_in[owner].astype(jnp.float32), jnp.zeros((per_owner, LANES - head), jnp.float32)], axis=1
+        )
         queries = [
             jnp.where(head_row == h, asked, 0.0).astype(jnp.bfloat16) for h in range(per_owner)
         ]
@@ -620,7 +619,7 @@
             pltpu.VMEM((n, per_owner, count), jnp.bfloat16),
             pltpu.VMEM((n, per_owner, count), jnp.bfloat16),
             pltpu.VMEM((per_owner, head), jnp.bfloat16),
-            pltpu.VMEM((n, per_owner, LANES), jnp.bfloat16),
+            pltpu.VMEM((n, per_owner, head), jnp.bfloat16),
             pltpu.VMEM((n, per_owner, LANES), jnp.bfloat16),
             pltpu.VMEM((n, per_owner, LANES), jnp.bfloat16),
             pltpu.VMEM((per_owner, LANES), jnp.float32),

time: 142 us -> 142 us (level)
  no operation moved by 1% of the time
where the time goes in v8:
time: 142 us
  Pallas kernels  142 us (100%)
    pallas_call x1, Pallas kernels, on_device(): pl.pallas_call(functools.partial(exchange_kernel, n, per_owner, tile, hea...  111 us
    pallas_call x1, Pallas kernels, on_device(): pl.pallas_call(functools.partial(rest_kernel, n, first_row), name='rest',...  27.1 us

profile of v8, /device:TPU:11, one launch (start us, length us, event | category | flops | bytes accessed | tf_op | source)
XLA Modules:
  0.0 142.2 jit_solution(12132576072287092528)
XLA Ops:
  0.6 110.9 %exchange.1 = (bf16[4,6144,128]{2,1,0:T(8,128)(2,1)S(1)}, bf16[8,4,768,128]{3,2,1,0:T(8,128)(2,1)S(1)}, f32[4,6144]{1,0:T(4,128)S(1)}, bf16[4,64]{1,0:T(4,128)(2,1)S(1)}) custom-call(bf16[768,2048]{1,0:T(8,128)(2,1)} %bitcast.7, bf16[2048,2048]{1,0:T(8,128)(2,1)} %key_weight.1, bf16[2048,2048]{1,0:T(8,128)(2,1)} %value_weight.1, f32[8,4,1,768]{3,2,1,0:T(1,128)} %bitcast.8, ...), custom_call_target="tpu_custom_call" | custom-call | tf_op jit(solution)/shard_map/exchange/pallas_call | solution.py:604
  111.5 2.2 %finish.1 = (bf16[4,6144,128]{2,1,0:T(8,128)(2,1)}, f32[4,6144]{1,0:T(4,128)}, bf16[4,64]{1,0:T(4,128)(2,1)}, f32[8,128]{1,0:T(8,128)S(1)}) custom-call(bf16[4,6144,128]{2,1,0:T(8,128)(2,1)S(1)} %get-tuple-element.12.kv, f32[4,6144]{1,0:T(4,128)S(1)} %get-tuple-element.13.gates, bf16[4,64]{1,0:T(4,128)(2,1)S(1)} %get-tuple-element.14.answer), custom_call_target="tpu_custom_call" | custom-call | tf_op jit(solution)/shard_map/finish/pallas_call | solution.py:658
  113.7 27.1 %rest.1.late = bf16[4,2048,128]{2,1,0:T(8,128)(2,1)S(1)} custom-call(bf16[8,4,768,128]{3,2,1,0:T(8,128)(2,1)S(1)} %get-tuple-element.11.outgoing, f32[8,128]{1,0:T(8,128)S(1)} %get-tuple-element.15.after), custom_call_target="tpu_custom_call" | custom-call | tf_op jit(solution)/shard_map/rest/pallas_call | solution.py:673
  140.8 1.4 last.1
